TPU v7x, 512 devices: a whole 4x4x16 slice. The times are simulated.
512 devices in a mesh: sp: 16 (over y, x), tp: 32 (over z, core).
Axes of the slice: x: 4, y: 4, z: 16, core: 2. Of those that a mesh axis runs over, the one named last changes fastest.
Arguments:
- stream: bfloat16 [8192, 4096], P('sp', 'tp'), may hold values from -6 to 6
- gain_first: bfloat16 [4096], P('tp'), may hold values from 0.099609375 to 1.8984375
- query_first: bfloat16 [4096, 4096], P('sp', 'tp'), may hold values from -0.09375 to 0.09375
- key_first: bfloat16 [4096, 4096], P('sp', 'tp'), may hold values from -0.09375 to 0.09375
- value_first: bfloat16 [4096, 4096], P('sp', 'tp'), may hold values from -0.09375 to 0.09375
- offset_first: float32 [32, 15, 31], P('tp'), may hold values from -4 to 254
- gain_second: bfloat16 [4096], P('tp'), may hold values from 0.099609375 to 1.8984375
- query_second: bfloat16 [4096, 4096], P('sp', 'tp'), may hold values from -0.09375 to 0.09375
- key_second: bfloat16 [4096, 4096], P('sp', 'tp'), may hold values from -0.09375 to 0.09375
- value_second: bfloat16 [4096, 4096], P('sp', 'tp'), may hold values from -0.09375 to 0.09375
- offset_second: float32 [32, 15, 31], P('tp'), may hold values from -4 to 254
Outputs:
- result: bfloat16 [8192, 4096], P('sp', 'tp')
All inputs are finite; a program needn't handle non-finite values.
Results may differ from a plain program's by a relative error of at most 0.008.
Values may be sent and summed in bfloat16 or wider, within the bound.
No kernel may reach another device: no remote copies, remote signals or barrier semaphores. Data moves between devices by JAX's collectives and lax.ppermute only.
A program may use at most 64 MiB of HBM per device.

v0:
```python
import jax
import jax.numpy as jnp
import numpy as np
from jax import lax
from jax.sharding import PartitionSpec as P

GRID_W = 64
epsilon = 1e-06


def turned_gather(arrays, axis, dims):
    turned = [jnp.moveaxis(a, dim, 0) for a, dim in zip(arrays, dims)]
    both = jnp.concatenate([t.reshape(len(t), -1) for t in turned], axis=1)
    filled, at, gathered = (lax.all_gather(both, axis, axis=0, tiled=True), 0, [])
    for t, dim in zip(turned, dims):
        section = filled[:, at : at + t[0].size].reshape(-1, *t.shape[1:])
        gathered.append(jnp.moveaxis(section, 0, dim))
        at += t[0].size
    return tuple(gathered)


def padded_2(block, sides, width):
    for axis, dim in sides:
        count = lax.axis_size(axis)
        forward = [(i, i + 1) for i in range(count - 1)]
        backward = [(target, source) for source, target in forward]
        low = lax.ppermute(
            lax.slice_in_dim(block, block.shape[dim] - width, None, axis=dim), axis, forward
        )
        high = lax.ppermute(lax.slice_in_dim(block, 0, width, axis=dim), axis, backward)
        block = jnp.concatenate([low, block, high], axis=dim)
    return block


def sent_together(arrays, axis, dim, along):
    ends, at = ([], 0)
    for a in arrays[:-1]:
        at += a.shape[along]
        ends.append(at)
    both = jnp.concatenate(arrays, axis=along)
    return tuple(jnp.split(lax.all_gather(both, axis, axis=dim, tiled=True), ends, axis=along))


def attend(query, keys, values, table, row_start, total_rows):
    rows_here, width, heads, head_size = query.shape
    blocks = width // 16
    query_cols = np.arange(width).reshape(blocks, 16)
    window_start = np.clip(query_cols - 8, 0, width - 16)
    key_cols = np.clip(np.arange(blocks) * 16 - 8, 0, width - 32)[:, None] + np.arange(32)
    column_ok = (key_cols[:, None, :] >= window_start[:, :, None]) & (
        key_cols[:, None, :] < window_start[:, :, None] + 16
    )
    column_offset = np.clip(key_cols[:, None, :] - query_cols[:, :, None] + 15, 0, 30)
    column_bias = table[:, :, column_offset]
    mask = jnp.asarray(column_ok)[None, :, :, None, :]
    factor = head_size ** (-0.5)

    def one_row(index):
        grid_row = row_start + index
        first = jnp.clip(grid_row - 4, 0, total_rows - 8)
        local = first - row_start + 4
        key_block = lax.dynamic_slice_in_dim(keys, local, 8, 0)[:, key_cols]
        value_block = lax.dynamic_slice_in_dim(values, local, 8, 0)[:, key_cols]
        query_row = lax.dynamic_index_in_dim(query, index, 0, keepdims=False).reshape(
            blocks, 16, heads, head_size
        )
        scores = (
            jnp.einsum(
                "jqhe,mjkhe->hjqmk", query_row, key_block, preferred_element_type=jnp.float32
            )
            * factor
        )
        row_offset = first + jnp.arange(8, dtype=jnp.int32) - grid_row + 7
        row_bias = jnp.transpose(jnp.take(column_bias, row_offset, axis=1), (0, 2, 3, 1, 4))
        scores = jnp.where(mask, scores + row_bias, -1e30)
        weight = jax.nn.softmax(scores.reshape(heads, blocks, 16, 256), axis=-1)
        rounded = weight.astype(jnp.bfloat16).reshape(heads, blocks, 16, 8, 32)
        output = jnp.einsum(
            "hjqmk,mjkhe->jqhe", rounded, value_block, preferred_element_type=jnp.float32
        )
        return output.reshape(width, heads * head_size)

    return jax.vmap(one_row)(jnp.arange(rows_here, dtype=jnp.int32))


def layer(stream, gain, table, whole_weights):
    tokens_dev, local_width = stream.shape
    widened = stream.astype(jnp.float32)
    full_rows, full_gain = turned_gather((stream, gain), "tp", (1, 0))
    full_wide = full_rows.astype(jnp.float32)
    mean_square = jnp.mean(full_wide * full_wide, axis=-1, keepdims=True)
    normed = (full_wide * lax.rsqrt(mean_square + epsilon) * full_gain.astype(jnp.float32)).astype(
        jnp.bfloat16
    )
    query = jnp.dot(normed, whole_weights[0], preferred_element_type=jnp.float32)
    key_part = jnp.dot(normed, whole_weights[1], preferred_element_type=jnp.float32)
    value_part = jnp.dot(normed, whole_weights[2], preferred_element_type=jnp.float32)
    heads_dev = table.shape[0]
    rows_dev = tokens_dev // GRID_W
    shape = (rows_dev, GRID_W, heads_dev, local_width // heads_dev)
    query = query.astype(jnp.bfloat16).reshape(shape)
    paired = jnp.stack(
        [
            key_part.astype(jnp.bfloat16).reshape(shape),
            value_part.astype(jnp.bfloat16).reshape(shape),
        ]
    )
    padded = padded_2(paired, (("sp", 1),), 4)
    row_start = lax.axis_index("sp") * rows_dev
    output = attend(query, padded[0], padded[1], table, row_start, rows_dev * lax.axis_size("sp"))
    return (widened + output.reshape(tokens_dev, local_width)).astype(jnp.bfloat16)


def body(
    stream,
    gain_first,
    query_first,
    key_first,
    value_first,
    offset_first,
    gain_second,
    query_second,
    key_second,
    value_second,
    offset_second,
):
    fetched = sent_together(
        (query_first, key_first, value_first, query_second, key_second, value_second), "sp", 0, 1
    )
    first_set = fetched[:3]
    second_set = fetched[3:]
    middle = layer(stream, gain_first, offset_first, first_set)
    return layer(middle, gain_second, offset_second, second_set)


def solution(mesh):
    placed = (
        P("sp", "tp"),
        P("tp"),
        P("sp", "tp"),
        P("sp", "tp"),
        P("sp", "tp"),
        P("tp", None, None),
        P("tp"),
        P("sp", "tp"),
        P("sp", "tp"),
        P("sp", "tp"),
        P("tp", None, None),
    )
    return jax.shard_map(body, mesh=mesh, in_specs=placed, out_specs=P("sp", "tp"), check_vma=False)
```

profile of v0, /device:TPU:6, one launch (start us, length us, event | category | flops | bytes accessed | tf_op | source)
XLA Modules:
  0.0 339.2 jit_solution(11450175371349849308)
XLA Ops:
  6.5 1.6 pad_maximum_fusion.2
  8.2 0.9 constant_dynamic-update-slice_fusion.5
  9.1 0.9 constant_dynamic-update-slice_fusion.4
  9.9 0.9 constant_dynamic-update-slice_fusion.3
  10.8 0.9 constant_dynamic-update-slice_fusion.2
  11.7 0.9 constant_dynamic-update-slice_fusion.1
  12.5 0.9 constant_dynamic-update-slice_fusion
  13.4 0.7 copy-done.3
  14.3 0.1 reshape.330
  14.4 0.8 copy.40
  15.2 0.7 broadcast_clamp_fusion
  15.9 5.5 %gather_fusion.5 = f32[2048,15]{1,0:T(8,128)S(1)} fusion(f32[15,31]{0,1:T(8,128)S(1)} %bitcast.128, s32[2048]{0:T(1024)S(1)} %broadcast_clamp_fusion), kind=kCustom, calls=%fused_computation.7 | custom fusion | bytes 253952 | tf_op jit(solution)/shard_map/gather | solution.py:54
  21.3 0.6 copy.41
  22.0 2.0 gather_fusion.12
  24.0 0.1 compare_and_fusion
  24.1 70.7 %all-gather.4.cloned.1.call-done = bf16[4096,513]{0,1:T(8,128)(2,1)} async-done(((bf16[128,513]{0,1:T(8,128)(2,1)}), bf16[4096,513]{0,1:T(8,128)(2,1)}) %all-gather.4.cloned.1.call-update) | async-done | bytes 4202512 | tf_op jit(solution)/shard_map/all_gather | solution.py:14
  94.8 3.1 fusion
  97.9 0.9 slice_convert_fusion.1
  98.7 5.9 %fusion.2 = bf16[4096,512]{0,1:T(8,128)(2,1)} fusion(f32[4096]{0:T(1024)S(1)} %bitcast.154, f32[512]{0:T(512)S(1)} %add_rsqrt_fusion.1, bf16[4096,513]{0,1:T(8,128)(2,1)} %all-gather.4.cloned.1.call-done), kind=kLoop, calls=%fused_computation.20 | loop fusion | flops 8388608 | bytes 8407040 | tf_op jit(solution)/shard_map/convert_element_type | solution.py:92
  104.6 65.2 %all-gather.6.cloned.1.call-done = bf16[4096,768]{1,0:T(8,128)(2,1)} async-done(((bf16[256,768]{1,0:T(8,128)(2,1)}), bf16[4096,768]{1,0:T(8,128)(2,1)}) %all-gather.6.cloned.1.call-update) | async-done | bytes 6291472 | tf_op jit(solution)/shard_map/all_gather | solution.py:41
  169.8 3.9 %convolution_convert_fusion.5 = bf16[512,128]{1,0:T(8,128)(2,1)S(1)} fusion(bf16[4096,512]{0,1:T(8,128)(2,1)} %fusion.2, bf16[4096,768]{1,0:T(8,128)(2,1)} %all-gather.6.cloned.1.call-done), kind=kOutput, calls=%fused_computation.53 | convolution fusion | flops 536936448 | bytes 5373952 | tf_op jit(solution)/shard_map/dot_general | solution.py:96
  173.7 2.5 convolution_convert_fusion.4
  176.2 3.3 collective-permute-start
  179.5 2.7 collective-permute-start.1
  182.3 2.5 convolution_convert_fusion.3
  184.7 0.6 gather_fusion.2
  185.3 3.2 collective-permute-done.1
  188.6 0.8 gather_fusion.3
  189.4 0.7 copy.38
  190.1 0.8 gather_fusion
  190.9 0.7 copy.34
  191.6 2.6 gather_fusion.4
  194.1 2.6 gather_fusion.1
  196.7 5.2 %fusion.41 = (f32[8,4,16]{2,1,0:T(4,128)S(1)}, f32[8,1,4,16,8,32]{5,3,4,2,0,1:T(8,128)S(1)}) fusion(f32[8,1,8,4,16,32]{5,4,3,2,0,1:T(8,128)} %bitcast.132, pred[8,8]{1,0:T(8,128)(4,1)S(1)} %compare_and_fusion, bf16[8,4,16,128,1]{3,2,4,1,0:T(8,128)(2,1)S(1)} %bitcast.142, bf16[4,32,8,8,128]{4,3,2,1,0:T(8,128)(2,1)} %bitcast.135, ...), kind=kOutput, calls=%fused_computation.105 | convolution fusion | flops 34209280 | bytes 3280960 | tf_op jit(solution)/shard_map/vmap(jqhe,mjkhe->hjqmk)/dot_general | solution.py:68
  201.9 0.5 fusion.20
  202.4 1.1 copy-done.2
  203.5 2.0 fusion.14
  205.5 0.7 pad_maximum_fusion.3
  206.2 0.1 copy.49
  206.3 5.6 %gather_fusion.11 = f32[2048,15]{1,0:T(8,128)S(1)} fusion(f32[15,31]{0,1:T(8,128)S(1)} %bitcast.129, s32[2048]{0:T(1024)S(1)} %broadcast_clamp_fusion), kind=kCustom, calls=%fused_computation.13 | custom fusion | bytes 253952 | tf_op jit(solution)/shard_map/gather | solution.py:54
  211.9 0.6 copy.50
  212.6 0.7 gather_fusion.13
  213.3 74.9 %all-gather.8.cloned.1.call-done = bf16[4096,513]{0,1:T(8,128)(2,1)} async-done(((bf16[128,513]{0,1:T(8,128)(2,1)}), bf16[4096,513]{0,1:T(8,128)(2,1)}) %all-gather.8.cloned.1.call-update) | async-done | bytes 4202512 | tf_op jit(solution)/shard_map/all_gather | solution.py:14
  288.1 3.2 fusion.3
  291.4 0.9 slice_convert_fusion
  292.2 4.0 %fusion.5 = bf16[4096,512]{0,1:T(8,128)(2,1)S(1)} fusion(f32[4096]{0:T(1024)S(1)} %bitcast.155, f32[512]{0:T(512)S(1)} %add_rsqrt_fusion, bf16[4096,513]{0,1:T(8,128)(2,1)} %all-gather.8.cloned.1.call-done), kind=kLoop, calls=%fused_computation.23 | loop fusion | flops 8388608 | bytes 8407040 | tf_op jit(solution)/shard_map/convert_element_type | solution.py:92
  296.2 1.2 convolution_convert_fusion.1
  297.5 1.2 convolution_convert_fusion.2
  298.8 3.4 collective-permute-start.2
  302.2 2.7 collective-permute-start.3
  304.9 1.2 convolution_convert_fusion
  306.1 1.2 gather_fusion.8
  307.4 4.1 %collective-permute-done.3 = bf16[2,4,64,1,128]{4,2,1,3,0:T(8,128)(2,1)S(1)} collective-permute-done((bf16[2,4,64,1,128]{4,2,1,3,0:T(8,128)(2,1)S(1)}, bf16[2,4,64,1,128]{4,2,1,3,0:T(8,128)(2,1)S(1)}, u32[]{:S(2)}, u32[]{:S(2)}) %collective-permute-start.3) | collective-permute-done | bytes 131104 | tf_op jit(solution)/shard_map/ppermute | solution.py:30
  311.6 1.7 gather_fusion.9
  313.3 1.9 copy.47
  315.2 2.5 gather_fusion.10
  317.8 1.6 gather_fusion.6
  319.4 1.9 copy.43
  321.4 2.5 gather_fusion.7
  323.9 4.5 %fusion.42 = (f32[8,4,16]{2,1,0:T(4,128)S(1)}, f32[8,1,4,16,8,32]{5,3,4,2,0,1:T(8,128)S(1)}) fusion(f32[8,1,8,4,16,32]{5,4,3,2,0,1:T(8,128)S(1)} %bitcast.133, pred[8,8]{1,0:T(8,128)(4,1)S(1)} %copy-done.9, bf16[8,4,16,128,1]{3,2,4,1,0:T(8,128)(2,1)S(1)} %bitcast.141, bf16[4,32,8,8,128]{4,3,2,1,0:T(8,128)(2,1)} %bitcast.134, ...), kind=kOutput, calls=%fused_computation.106 | convolution fusion | flops 34209280 | bytes 3280960 | tf_op jit(solution)/shard_map/vmap(jqhe,mjkhe->hjqmk)/dot_general | solution.py:68
  328.4 0.5 fusion.21
  329.0 1.1 copy-done.1
  330.0 2.0 fusion.9
  332.0 0.7 fusion.36
  (51 shorter events, 0.6 us)
Async XLA Ops:
  6.5 88.3 %all-gather.4.cloned.1.call-start = ((), (), s32[]{:S(2)}) async-start(), calls=%async_computation | async-start | bytes 4392960 | tf_op jit(solution)/shard_map/all_gather | solution.py:14
  8.2 161.6 %all-gather.6.cloned.1.call-start = ((), (), s32[]{:S(2)}) async-start(), calls=%async_computation.1 | async-start | bytes 6684672 | tf_op jit(solution)/shard_map/all_gather | solution.py:41
  13.4 0.7 copy-start.3
  14.2 274.0 %all-gather.8.cloned.1.call-start = ((), (), s32[]{:S(2)}) async-start(), calls=%async_computation.2 | async-start | bytes 4392960 | tf_op jit(solution)/shard_map/all_gather | solution.py:14
  22.0 2.0 copy-start.12
  24.1 172.6 %copy-start.8 = (pred[8,8]{1,0:T(8,128)(4,1)}, pred[8,8]{1,0:T(8,128)(4,1)S(1)}, u32[]{:S(2)}) copy-start(pred[8,8]{1,0:T(8,128)(4,1)S(1)} %compare_and_fusion) | copy-start | bytes 196
  169.8 3.9 %copy-start = (bf16[4096,512]{0,1:T(8,128)(2,1)S(1)}, bf16[4096,512]{0,1:T(8,128)(2,1)}, u32[]{:S(2)}) copy-start(bf16[4096,512]{0,1:T(8,128)(2,1)} %fusion.2) | copy-start | bytes 12582916
  176.2 9.1 %collective-permute-start = (bf16[2,4,64,1,128]{4,2,1,3,0:T(8,128)(2,1)S(1)}, bf16[2,4,64,1,128]{4,2,1,3,0:T(8,128)(2,1)S(1)}, u32[]{:S(2)}, u32[]{:S(2)}) collective-permute-start(bf16[2,4,64,1,128]{4,2,1,3,0:T(8,128)(2,1)S(1)} %get-tuple-element.12), channel_id=1, source_target_pairs={{0,32},{32,64},{64,96},{96,128},{128,160},{160,192},{192,224},{224... | collective-permute-start | bytes 393224 | tf_op jit(solution)/shard_map/ppermute | solution.py:27
  179.5 9.0 %collective-permute-start.1 = (bf16[2,4,64,1,128]{4,2,1,3,0:T(8,128)(2,1)S(1)}, bf16[2,4,64,1,128]{4,2,1,3,0:T(8,128)(2,1)S(1)}, u32[]{:S(2)}, u32[]{:S(2)}) collective-permute-start(bf16[2,4,64,1,128]{4,2,1,3,0:T(8,128)(2,1)S(1)} %get-tuple-element.13), channel_id=1, source_target_pairs={{32,0},{64,32},{96,64},{128,96},{160,128},{192,160},{224,192},{256... | collective-permute-start | bytes 393224 | tf_op jit(solution)/shard_map/ppermute | solution.py:30
  194.1 2.6 copy-start.6
  201.9 1.6 copy-start.2
  203.5 2.0 copy-start.5
  203.5 2.0 copy-start.11
  203.5 2.7 copy-start.10
  288.1 8.1 %slice-start = ((s8[6291456]{0:T(1024)(128)(4,1)}), s8[4194304]{0:T(1024)(128)(4,1)S(1)}, s32[]{:S(2)}) async-start(s8[6291456]{0:T(1024)(128)(4,1)} %bitcast.158), calls=%async_computation.3 | async-start | bytes 8388608
  292.2 4.0 %slice-start.1 = ((s8[6291456]{0:T(1024)(128)(4,1)}), s8[2097152]{0:T(1024)(128)(4,1)S(1)}, s32[]{:S(2)}) async-start(s8[6291456]{0:T(1024)(128)(4,1)} %bitcast.158), calls=%async_computation.4 | async-start | bytes 4194304
  298.8 8.6 %collective-permute-start.2 = (bf16[2,4,64,1,128]{4,2,1,3,0:T(8,128)(2,1)S(1)}, bf16[2,4,64,1,128]{4,2,1,3,0:T(8,128)(2,1)S(1)}, u32[]{:S(2)}, u32[]{:S(2)}) collective-permute-start(bf16[2,4,64,1,128]{4,2,1,3,0:T(8,128)(2,1)S(1)} %get-tuple-element.10), channel_id=1, source_target_pairs={{0,32},{32,64},{64,96},{96,128},{128,160},{160,192},{192,224},{224... | collective-permute-start | bytes 393224 | tf_op jit(solution)/shard_map/ppermute | solution.py:27
  302.2 9.4 %collective-permute-start.3 = (bf16[2,4,64,1,128]{4,2,1,3,0:T(8,128)(2,1)S(1)}, bf16[2,4,64,1,128]{4,2,1,3,0:T(8,128)(2,1)S(1)}, u32[]{:S(2)}, u32[]{:S(2)}) collective-permute-start(bf16[2,4,64,1,128]{4,2,1,3,0:T(8,128)(2,1)S(1)} %get-tuple-element.11), channel_id=1, source_target_pairs={{32,0},{64,32},{96,64},{128,96},{160,128},{192,160},{224,192},{256... | collective-permute-start | bytes 393224 | tf_op jit(solution)/shard_map/ppermute | solution.py:30
  321.3 2.6 copy-start.4
  321.3 2.5 copy-start.7
  321.3 2.5 copy-start.9
  328.4 1.6 copy-start.1
Sparse Core Ops, SparseCore 0:
  9.4 85.3 all-gather.3
  97.8 71.9 all-gather.5
  206.4 81.7 all-gather.7
where the time goes:
time: 340 us; the launch traced here: 339 us
  waiting for transfers between devices  218 us (64%)
  local copies, waits for them, and re-layouts  46.2 us (14%)
  matrix products  26.2 us (8%)
  other arithmetic  23.1 us (7%)
  between operations  13.5 us (4%)
  starting transfers between devices  12.2 us (4%)
    all_gather x2, waiting for transfers between devices, turned_gather(): lax.all_gather(both, axis, axis=0, tiled=True)  146 us
    all_gather x1, waiting for transfers between devices, sent_together(): lax.all_gather(both, axis, axis=dim, tiled=True)  65.2 us
    gather x4, local copies, waits for them, and re-layouts, attend(): column_bias = table[:, :, column_offset]  12.3 us
    gather x6, local copies, waits for them, and re-layouts, one_row(): key_block = lax.dynamic_slice_in_dim(keys, local, 8, 0)[:, key_cols]  10.2 us
    gather x6, local copies, waits for them, and re-layouts, one_row(): value_block = lax.dynamic_slice_in_dim(values, local, 8, 0)[:, key_cols]  10.1 us
    convert_element_type x2, other arithmetic, layer(): (full_wide * lax.rsqrt(mean_square + epsilon) * full_gain.astype(jnp.floa...  9.88 us
    dot_general x2, matrix products, one_row(): jnp.einsum('jqhe,mjkhe->hjqmk', query_row, key_block, preferred_element_t...  9.71 us
    unnamed x37, local copies, waits for them, and re-layouts  8.13 us
  transfers between devices with their start and end apart: 7, of which 5 were waited for; matrix products, arithmetic and copies ran while one was open for 11% of the time, Pallas kernels for 0%

commit v1 on v0

--- a/solution.py
+++ b/solution.py
@@ -11,7 +11,13 @@
 def turned_gather(arrays, axis, dims):
     turned = [jnp.moveaxis(a, dim, 0) for a, dim in zip(arrays, dims)]
     both = jnp.concatenate([t.reshape(len(t), -1) for t in turned], axis=1)
-    filled, at, gathered = (lax.all_gather(both, axis, axis=0, tiled=True), 0, [])
+    filled, at, gathered = (
+        jnp.concatenate(
+            lax.all_to_all(jnp.stack([both] * lax.axis_size(axis)), axis, 0, 0), axis=0
+        ),
+        0,
+        [],
+    )
     for t, dim in zip(turned, dims):
         section = filled[:, at : at + t[0].size].reshape(-1, *t.shape[1:])
         gathered.append(jnp.moveaxis(section, 0, dim))

time: 340 us -> 535 us (1.57)
  the two profiles are of different devices: /device:TPU:6 before, /device:TPU:46 now
where the time goes in v1:
time: 535 us; the launch traced here: 525 us
  waiting for transfers between devices  374 us (70%)
  local copies, waits for them, and re-layouts  65.3 us (12%)
  starting transfers between devices  32.9 us (6%)
  matrix products  26.5 us (5%)
  between operations  14.2 us (3%)
  other arithmetic  12.3 us (2%)
    all_to_all x2, waiting for transfers between devices, turned_gather(): lax.all_to_all(jnp.stack([both] * lax.axis_size(axis)), axis, 0, 0)  368 us
    all_to_all x2, starting transfers between devices, turned_gather(): lax.all_to_all(jnp.stack([both] * lax.axis_size(axis)), axis, 0, 0)  20.5 us
    gather x6, local copies, waits for them, and re-layouts, one_row(): key_block = lax.dynamic_slice_in_dim(keys, local, 8, 0)[:, key_cols]  12.4 us
    gather x6, local copies, waits for them, and re-layouts, one_row(): value_block = lax.dynamic_slice_in_dim(values, local, 8, 0)[:, key_cols]  12.3 us
    gather x4, local copies, waits for them, and re-layouts, attend(): column_bias = table[:, :, column_offset]  12.1 us
    unnamed x53, local copies, waits for them, and re-layouts  11.5 us
  transfers between devices with their start and end apart: 7, of which 4 were waited for; matrix products, arithmetic and copies ran while one was open for 6% of the time, Pallas kernels for 0%

profile of v1, /device:TPU:46, one launch (start us, length us, event | category | flops | bytes accessed | tf_op | source)
XLA Modules:
  0.0 525.1 jit_solution(4771322932335678813)
XLA Ops:
  6.5 0.9 pad_maximum_fusion.2
  7.5 2.6 stack.8
  10.1 15.5 %all-to-all-start = ((bf16[32,128,513]{1,2,0:T(8,128)(2,1)}), bf16[32,128,513]{1,2,0:T(8,128)(2,1)}, u32[]{:S(2)}, u32[]{:S(2)}) async-start(bf16[32,128,513]{1,2,0:T(8,128)(2,1)} %stack.8), calls=%async_computation | async-start | bytes 8519680 | tf_op jit(solution)/shard_map/all_to_all | solution.py:16
  26.0 0.7 copy-done.1
  27.0 5.5 %gather_fusion.5 = f32[2048,15]{1,0:T(8,128)S(1)} fusion(f32[15,31]{0,1:T(8,128)S(1)} %bitcast.142, s32[2048]{0:T(1024)S(1)} %broadcast_clamp_fusion), kind=kCustom, calls=%fused_computation.7 | custom fusion | bytes 253952 | tf_op jit(solution)/shard_map/gather | solution.py:60
  32.5 0.6 copy.82
  33.1 0.6 pad_clamp_fusion
  33.7 0.7 gather_fusion.12
  34.5 0.6 compare_and_fusion
  35.1 183.5 %all-to-all-done = bf16[32,128,513]{1,2,0:T(8,128)(2,1)} async-done(((bf16[32,128,513]{1,2,0:T(8,128)(2,1)}), bf16[32,128,513]{1,2,0:T(8,128)(2,1)}, u32[]{:S(2)}, u32[]{:S(2)}) %all-to-all-start) | async-done | bytes 4202528 | tf_op jit(solution)/shard_map/all_to_all | solution.py:16
  218.6 2.8 copy.135
  221.4 0.7 pad.28
  222.1 4.2 copy.100
  226.4 0.9 fusion
  227.3 3.7 fusion.2
  231.0 3.9 convolution_convert_fusion.5
  234.9 2.5 convolution_convert_fusion.4
  237.4 3.4 collective-permute-start
  240.8 2.9 collective-permute-start.1
  243.7 2.5 convolution_convert_fusion.3
  246.2 0.6 gather_fusion.2
  246.8 3.0 collective-permute-done.1
  249.9 1.7 gather_fusion.3
  251.5 1.9 copy.79
  253.5 2.7 gather_fusion.4
  256.2 4.5 fusion.39
  260.7 0.5 fusion.20
  261.2 0.5 fusion.32
  261.7 1.4 copy.84
  263.1 1.7 gather_fusion
  264.7 1.9 copy.75
  266.7 2.6 gather_fusion.1
  269.2 2.4 fusion.14
  271.8 2.6 stack.10
  274.4 4.9 all-to-all-start.1
  279.4 5.5 %gather_fusion.11 = f32[2048,15]{1,0:T(8,128)S(1)} fusion(f32[15,31]{0,1:T(8,128)S(1)} %bitcast.143, s32[2048]{0:T(1024)S(1)} %broadcast_clamp_fusion), kind=kCustom, calls=%fused_computation.13 | custom fusion | bytes 253952 | tf_op jit(solution)/shard_map/gather | solution.py:60
  284.9 0.6 copy.93
  285.5 0.7 gather_fusion.13
  286.2 184.4 %all-to-all-done.1 = bf16[32,128,513]{1,2,0:T(8,128)(2,1)} async-done(((bf16[32,128,513]{1,2,0:T(8,128)(2,1)}), bf16[32,128,513]{1,2,0:T(8,128)(2,1)}, u32[]{:S(2)}, u32[]{:S(2)}) %all-to-all-start.1) | async-done | bytes 4202528 | tf_op jit(solution)/shard_map/all_to_all | solution.py:16
  470.6 2.8 copy.134
  473.5 0.7 pad.29
  474.2 4.2 copy.101
  478.5 0.9 fusion.3
  479.4 1.7 fusion.5
  481.1 0.5 slice-done.1
  481.6 1.2 convolution_convert_fusion.1
  482.8 1.2 convolution_convert_fusion.2
  484.1 2.6 collective-permute-start.2
  486.7 3.5 collective-permute-start.3
  490.2 1.2 convolution_convert_fusion
  491.4 1.2 gather_fusion.8
  492.7 3.0 collective-permute-done.3
  495.8 1.7 gather_fusion.9
  497.5 1.9 copy.90
  499.4 2.5 gather_fusion.10
  501.9 4.5 fusion.40
  506.5 0.5 fusion.21
  507.0 0.5 fusion.33
  507.5 1.4 copy.95
  508.8 1.7 gather_fusion.6
  510.5 1.9 copy.86
  512.4 2.5 gather_fusion.7
  515.0 2.4 fusion.9
  517.3 0.7 fusion.34
  (73 shorter events, 1.0 us)
Async XLA Ops:
  10.1 15.7 %copy-start.3 = (bf16[256,128]{1,0:T(8,128)(2,1)S(1)}, bf16[256,128]{1,0:T(8,128)(2,1)}, u32[]{:S(2)}) copy-start(bf16[256,128]{1,0:T(8,128)(2,1)} %param.27) | copy-start | bytes 196612
  10.1 15.7 %copy-start.4 = (bf16[256,128]{1,0:T(8,128)(2,1)S(1)}, bf16[256,128]{1,0:T(8,128)(2,1)}, u32[]{:S(2)}) copy-start(bf16[256,128]{1,0:T(8,128)(2,1)} %param.28) | copy-start | bytes 196612
  10.1 15.7 %copy-start.5 = (bf16[256,128]{1,0:T(8,128)(2,1)S(1)}, bf16[256,128]{1,0:T(8,128)(2,1)}, u32[]{:S(2)}) copy-start(bf16[256,128]{1,0:T(8,128)(2,1)} %param.29) | copy-start | bytes 196612
  10.1 15.8 %copy-start.6 = (bf16[256,128]{1,0:T(8,128)(2,1)S(1)}, bf16[256,128]{1,0:T(8,128)(2,1)}, u32[]{:S(2)}) copy-start(bf16[256,128]{1,0:T(8,128)(2,1)} %param.32) | copy-start | bytes 196612
  10.1 15.8 %copy-start.7 = (bf16[256,128]{1,0:T(8,128)(2,1)S(1)}, bf16[256,128]{1,0:T(8,128)(2,1)}, u32[]{:S(2)}) copy-start(bf16[256,128]{1,0:T(8,128)(2,1)} %param.33) | copy-start | bytes 196612
  10.1 15.8 %copy-start.8 = (bf16[256,128]{1,0:T(8,128)(2,1)S(1)}, bf16[256,128]{1,0:T(8,128)(2,1)}, u32[]{:S(2)}) copy-start(bf16[256,128]{1,0:T(8,128)(2,1)} %param.34) | copy-start | bytes 196612
  10.1 16.8 %copy-start.15 = (f32[1,15,31]{2,0,1:T(1,128)S(1)}, f32[1,15,31]{2,0,1:T(1,128)}, u32[]{:S(2)}) copy-start(f32[1,15,31]{2,0,1:T(1,128)} %param.30) | copy-start | bytes 5584
  10.1 16.9 %copy-start.14 = (s32[2048]{0:T(1024)S(1)}, s32[2048]{0:T(1024)}, u32[]{:S(2)}) copy-start(s32[2048]{0:T(1024)} %constant.254) | copy-start | bytes 24580
  10.1 208.4 %all-to-all-start = ((bf16[32,128,513]{1,2,0:T(8,128)(2,1)}), bf16[32,128,513]{1,2,0:T(8,128)(2,1)}, u32[]{:S(2)}, u32[]{:S(2)}) async-start(bf16[32,128,513]{1,2,0:T(8,128)(2,1)} %stack.8), calls=%async_computation | async-start | bytes 8519680 | tf_op jit(solution)/shard_map/all_to_all | solution.py:16
  25.7 205.3 %all-gather.2.cloned.1.call-start = ((), (), s32[]{:S(2)}) async-start(), calls=%async_computation.2 | async-start | bytes 6684672 | tf_op jit(solution)/shard_map/all_gather | solution.py:47
  26.0 0.8 copy-start.1
  27.0 6.1 %copy-start.18 = (s32[128]{0:T(128)S(1)}, s32[128]{0:T(128)}, u32[]{:S(2)}) copy-start(s32[128]{0:T(128)} %constant.240) | copy-start | bytes 1540
  33.7 0.7 copy-start.11
  231.0 3.9 copy-start
  237.4 9.4 %collective-permute-start = (bf16[2,4,64,1,128]{4,2,1,3,0:T(8,128)(2,1)S(1)}, bf16[2,4,64,1,128]{4,2,1,3,0:T(8,128)(2,1)S(1)}, u32[]{:S(2)}, u32[]{:S(2)}) collective-permute-start(bf16[2,4,64,1,128]{4,2,1,3,0:T(8,128)(2,1)S(1)} %get-tuple-element.12), channel_id=1, source_target_pairs={{0,32},{32,64},{64,96},{96,128},{128,160},{160,192},{192,224},{224... | collective-permute-start | bytes 393224 | tf_op jit(solution)/shard_map/ppermute | solution.py:33
  240.8 9.0 %collective-permute-start.1 = (bf16[2,4,64,1,128]{4,2,1,3,0:T(8,128)(2,1)S(1)}, bf16[2,4,64,1,128]{4,2,1,3,0:T(8,128)(2,1)S(1)}, u32[]{:S(2)}, u32[]{:S(2)}) collective-permute-start(bf16[2,4,64,1,128]{4,2,1,3,0:T(8,128)(2,1)S(1)} %get-tuple-element.13), channel_id=1, source_target_pairs={{32,0},{64,32},{96,64},{128,96},{160,128},{192,160},{224,192},{256... | collective-permute-start | bytes 393224 | tf_op jit(solution)/shard_map/ppermute | solution.py:36
  263.1 3.6 copy-start.9
  269.2 2.4 copy-start.2
  269.2 2.5 copy-start.17
  274.4 5.0 copy-start.16
  274.4 196.3 %all-to-all-start.1 = ((bf16[32,128,513]{1,2,0:T(8,128)(2,1)}), bf16[32,128,513]{1,2,0:T(8,128)(2,1)}, u32[]{:S(2)}, u32[]{:S(2)}) async-start(bf16[32,128,513]{1,2,0:T(8,128)(2,1)} %stack.10), calls=%async_computation.1 | async-start | bytes 8519680 | tf_op jit(solution)/shard_map/all_to_all | solution.py:16
  279.4 6.1 %copy-start.12 = (s32[1024]{0:T(1024)S(1)}, s32[1024]{0:T(1024)}, u32[]{:S(2)}) copy-start(s32[1024]{0:T(1024)} %copy-done.11) | copy-start | bytes 12292
  478.5 2.6 slice-start
  479.4 2.2 slice-start.1
  484.1 8.6 %collective-permute-start.2 = (bf16[2,4,64,1,128]{4,2,1,3,0:T(8,128)(2,1)S(1)}, bf16[2,4,64,1,128]{4,2,1,3,0:T(8,128)(2,1)S(1)}, u32[]{:S(2)}, u32[]{:S(2)}) collective-permute-start(bf16[2,4,64,1,128]{4,2,1,3,0:T(8,128)(2,1)S(1)} %get-tuple-element.10), channel_id=1, source_target_pairs={{0,32},{32,64},{64,96},{96,128},{128,160},{160,192},{192,224},{224... | collective-permute-start | bytes 393224 | tf_op jit(solution)/shard_map/ppermute | solution.py:33
  486.7 9.0 %collective-permute-start.3 = (bf16[2,4,64,1,128]{4,2,1,3,0:T(8,128)(2,1)S(1)}, bf16[2,4,64,1,128]{4,2,1,3,0:T(8,128)(2,1)S(1)}, u32[]{:S(2)}, u32[]{:S(2)}) collective-permute-start(bf16[2,4,64,1,128]{4,2,1,3,0:T(8,128)(2,1)S(1)} %get-tuple-element.11), channel_id=1, source_target_pairs={{32,0},{64,32},{96,64},{128,96},{160,128},{192,160},{224,192},{256... | collective-permute-start | bytes 393224 | tf_op jit(solution)/shard_map/ppermute | solution.py:36
  495.8 3.6 copy-start.10
  499.4 2.5 copy-start.13
Sparse Core Ops, SparseCore 0:
  29.5 75.7 all-gather.1
